TPU v7x, 128 devices: a whole 4x4x4 slice. The times are simulated.
128 devices in a mesh: fs: 16 (over z, x), tp: 8 (over y, core).
Axes of the slice: x: 4, y: 4, z: 4, core: 2. Of those that a mesh axis runs over, the one named last changes fastest.
Arguments:
- h_saved: bfloat16 [32768, 2048], P('fs'), may hold values from -6 to 6
- conv_cotan: bfloat16 [32768, 2560], P('fs', 'tp'), may hold values from -64 to 64
- lru_out: bfloat16 [32768, 2560], P('fs', 'tp'), may hold values from -64 to 64
- out_cotan: bfloat16 [32768, 2048], P('fs'), may hold values from -6 to 6
- basis_in: bfloat16 [2048, 256], P('fs'), may hold values from -1.41421356 to 1.41421356
- basis_out: bfloat16 [2048, 256], P('fs'), may hold values from -1.41421356 to 1.41421356
- weight_in: float32 [2048, 2560], P('fs', 'tp'), may hold values from -0.125 to 0.125
- weight_out: float32 [2560, 2048], P('tp', 'fs'), may hold values from -0.125 to 0.125
- first_in: float32 [256, 2560], P('fs', 'tp'), may hold values from -6 to 6
- second_in: float32 [256, 2560], P('fs', 'tp'), may hold values from 0.05 to 2
- first_out: float32 [256, 2560], P('fs', 'tp'), may hold values from -6 to 6
- second_out: float32 [256, 2560], P('fs', 'tp'), may hold values from 0.05 to 2
Outputs:
- step_in: float32 [2048, 2560], P('fs', 'tp')
- new_weight_in: float32 [2048, 2560], P('fs', 'tp')
- copy_in: bfloat16 [2048, 2560], P(None, 'tp')
- new_first_in: float32 [256, 2560], P('fs', 'tp')
- new_second_in: float32 [256, 2560], P('fs', 'tp')
- step_out: float32 [2560, 2048], P('tp', 'fs')
- new_weight_out: float32 [2560, 2048], P('tp', 'fs')
- copy_out: bfloat16 [2560, 2048], P('tp')
- new_first_out: float32 [256, 2560], P('fs', 'tp')
- new_second_out: float32 [256, 2560], P('fs', 'tp')
All inputs are finite; a program needn't handle non-finite values.
Results may differ from a plain program's by a relative error of at most 0.0046.
Values may be sent and summed in bfloat16 or wider, within the bound.
No kernel may reach another device: no remote copies, remote signals or barrier semaphores. Data moves between devices by JAX's collectives and lax.ppermute only.
A program may use at most 128 MiB of HBM per device.

v0:
```python
import math
import jax
import jax.numpy as jnp
from jax import lax
from jax.sharding import Mesh
from jax.sharding import PartitionSpec as P

D_RNN = 2560
RANK = 256
FS = ("fs_0", "fs_1")
FS_TP = ("fs_0", "fs_1", "tp_0", "tp_1")
TP = ("tp_0", "tp_1")


def laid_out(blocks, dim):
    blocks = jnp.moveaxis(blocks, 0, dim)
    lengths = blocks.shape
    return blocks.reshape(*lengths[:dim], lengths[dim] * lengths[dim + 1], *lengths[dim + 2 :])


def sent_to_all(array, axis):
    copies = jnp.broadcast_to(array, (lax.axis_size(axis), *array.shape))
    return lax.all_to_all(copies, axis, split_axis=0, concat_axis=0, tiled=True)


def gather_directly(array, axis, dim):
    return laid_out(sent_to_all(array, axis), dim)


def in_one_piece(arrays, axis, dim, along):
    ends, at = ([], 0)
    for a in arrays[:-1]:
        at += a.shape[along]
        ends.append(at)
    both = jnp.concatenate(arrays, axis=along)
    return tuple(jnp.split(gather_directly(both, axis, dim), ends, axis=along))


def split_up(array, dim, size):
    lengths = array.shape
    blocks = array.reshape(*lengths[:dim], size, lengths[dim] // size, *lengths[dim + 1 :])
    return jnp.moveaxis(blocks, dim, 0)


def sent_and_summed(array, axis, dim):
    blocks = split_up(array, dim, lax.axis_size(axis))
    arrived = lax.all_to_all(blocks, axis, split_axis=0, concat_axis=0, tiled=True)
    return arrived.sum(axis=0)


def sent_together(arrays, axis, dim, along):
    both = jnp.concatenate(arrays, axis=along)
    filled, at, done = (sent_and_summed(both, axis, dim), 0, [])
    for a in arrays:
        done.append(lax.slice_in_dim(filled, at, at + a.shape[along], axis=along))
        at += a.shape[along]
    return tuple(done)


def by_axis(array, axes):
    for axis in axes:
        array = lax.psum(array, axis)
    return array


def in_one_piece_2(arrays, axis, dim, along):
    widths = [a.shape[along] for a in arrays]
    both = jnp.concatenate(arrays, axis=along)
    filled = lax.all_gather(both, axis, axis=dim, tiled=True)
    return tuple(jnp.split(filled, [sum(widths[:k]) for k in range(1, len(widths))], axis=along))


def turned_gather(arrays, axis, dims):
    turned = [jnp.moveaxis(a, dim, 0) for a, dim in zip(arrays, dims)]
    widths = [t[0].size for t in turned]
    both = jnp.concatenate([t.reshape(-1, w) for t, w in zip(turned, widths)], axis=1)
    filled = lax.all_gather(both, axis, axis=0, tiled=True)
    blocks = jnp.split(filled, [sum(widths[:k]) for k in range(1, len(widths))], axis=1)
    return tuple(
        (
            jnp.moveaxis(b.reshape(-1, *t.shape[1:]), 0, dim)
            for b, t, dim in zip(blocks, turned, dims)
        )
    )


def split_product(narrow, wide):
    upper = lax.optimization_barrier(wide.astype(jnp.bfloat16))
    lower = (wide - upper.astype(jnp.float32)).astype(jnp.bfloat16)
    turned = jnp.transpose(narrow)
    first_part = jnp.dot(turned, upper, preferred_element_type=jnp.float32)
    second_part = jnp.dot(turned, lower, preferred_element_type=jnp.float32)
    return first_part + second_part


def moments(proj, factor, first, second):
    scaled = factor * proj
    first_new = 0.8 * first + 0.2 * scaled
    second_new = 0.9 * second + 0.1 * scaled * scaled
    direction = (first_new / (jnp.sqrt(second_new) + 1e-08)).astype(jnp.bfloat16)
    return (first_new, second_new, direction)


def shards(
    h_saved,
    conv_cotan,
    lru_out,
    out_cotan,
    basis_in,
    basis_out,
    weight_in,
    weight_out,
    first_in,
    second_in,
    first_out,
    second_out,
):
    pairs = ((h_saved, conv_cotan), (out_cotan, lru_out))
    partial_value = []
    wholes = in_one_piece((basis_in, basis_out), FS, 0, 1)
    for number in range(2):
        reduced = jnp.dot(pairs[number][0], wholes[number], preferred_element_type=jnp.float32)
        partial_value.append(split_product(pairs[number][1], reduced).T)
    proj_in, proj_out = sent_together((partial_value[0], partial_value[1]), FS, 0, 1)
    total = by_axis(jnp.sum(proj_in * proj_in) + jnp.sum(proj_out * proj_out), FS_TP)
    factor = math.sqrt(2.0 * RANK * D_RNN) * lax.rsqrt(total + 1e-06)
    first_a, second_a, dir_in = moments(proj_in, factor, first_in, second_in)
    first_b, second_b, dir_out = moments(proj_out, factor, first_out, second_out)
    full_in, full_out = in_one_piece_2((dir_in, dir_out), FS, 0, 1)
    step_in = jnp.dot(basis_in, full_in, preferred_element_type=jnp.float32)
    step_out = jnp.dot(basis_out, full_out, preferred_element_type=jnp.float32).T
    new_in = weight_in - 0.02 * step_in
    new_out = weight_out - 0.02 * step_out
    copy_in, copy_out = turned_gather(
        (new_in.astype(jnp.bfloat16), new_out.astype(jnp.bfloat16)), FS, (0, 1)
    )
    return (
        step_in,
        new_in,
        copy_in,
        first_a,
        second_a,
        step_out,
        new_out,
        copy_out,
        first_b,
        second_b,
    )


def solution(mesh):
    finer = Mesh(mesh.devices.reshape(4, 4, 4, 2), ("fs_0", "fs_1", "tp_0", "tp_1"))
    placed = (
        P(FS, None),
        P(FS, TP),
        P(FS, TP),
        P(FS, None),
        P(FS, None),
        P(FS, None),
        P(FS, TP),
        P(TP, FS),
        P(FS, TP),
        P(FS, TP),
        P(FS, TP),
        P(FS, TP),
    )
    return jax.shard_map(
        shards,
        mesh=finer,
        in_specs=placed,
        out_specs=(
            P(FS, TP),
            P(FS, TP),
            P(None, TP),
            P(FS, TP),
            P(FS, TP),
            P(TP, FS),
            P(TP, FS),
            P(TP, None),
            P(FS, TP),
            P(FS, TP),
        ),
        check_vma=False,
    )
```

profile of v0, /device:TPU:0, one launch (start us, length us, event | category | flops | bytes accessed | tf_op | source)
XLA Modules:
  0.0 189.7 jit_solution(8411399123699626168)
XLA Ops:
  7.2 1.0 pad_maximum_fusion.2
  8.4 36.4 %all_to_all.10 = bf16[16,128,512]{2,1,0:T(8,128)(2,1)S(1)} all-to-all(bf16[16,128,512]{2,1,0:T(8,128)(2,1)S(1)} %broadcast_in_dim.3), channel_id=1, replica_groups=mesh['fs_0'=4,'fs_1'=4,'tp_0'=4,'tp_1'=2] {'fs_0','fs_1'}, dimensions={0} | all-to-all | bytes 4194304 | tf_op jit(solution)/shard_map/all_to_all | solution.py:23
  44.9 5.9 %fusion.10 = (bf16[2048,256]{0,1:T(8,128)(2,1)S(1)}, f32[2048,256]{0,1:T(8,128)S(1)}) fusion(bf16[2048,2048]{1,0:T(8,128)(2,1)} %param.15, bf16[2048,512]{1,0:T(8,128)(2,1)S(1)} %bitcast.23), kind=kOutput, calls=%fused_computation.33 | convolution fusion | flops 2148007936 | bytes 12582912 | tf_op jit(solution)/shard_map/dot_general | solution.py:122
  50.8 2.4 %fusion.11 = (bf16[2048,256]{0,1:T(8,128)(2,1)S(1)}, f32[2048,256]{0,1:T(8,128)S(1)}) fusion(bf16[2048,2048]{1,0:T(8,128)(2,1)S(1)} %bitcast.26, bf16[2048,512]{1,0:T(8,128)(2,1)S(1)} %bitcast.24), kind=kOutput, calls=%fused_computation.34 | convolution fusion | flops 2148007936 | bytes 12582912 | tf_op jit(solution)/shard_map/dot_general | solution.py:122
  53.2 0.5 fusion.13
  53.8 0.6 convolution_add_fusion
  54.4 0.7 copy-done.1
  55.1 0.5 fusion.12
  55.6 0.6 convolution_add_fusion.1
  56.4 0.2 copy.22
  56.6 15.2 %all_to_all.11 = f32[16,16,640]{2,1,0:T(8,128)S(1)} all-to-all(f32[16,16,640]{2,1,0:T(8,128)S(1)} %bitcast.22), channel_id=1, replica_groups=mesh['fs_0'=4,'fs_1'=4,'tp_0'=4,'tp_1'=2] {'fs_0','fs_1'}, dimensions={0} | all-to-all | bytes 1310720 | tf_op jit(solution)/shard_map/all_to_all | solution.py:47
  71.9 0.7 multiply_reduce_fusion
  73.9 9.1 %psum.28 = f32[]{:T(128)} all-reduce(f32[]{:T(128)S(6)} %add.42), channel_id=1, replica_groups=mesh['fs_0'=4,'fs_1'=4,'tp_0'=4,'tp_1'=2] {'fs_0'}, use_global_device_ids=true, to_apply=%region_3.0 | all-reduce | flops 1 | bytes 8 | tf_op jit(solution)/shard_map/psum | solution.py:62
  83.0 9.6 %psum.29 = f32[]{:T(128)} all-reduce(f32[]{:T(128)} %psum.28), channel_id=1, replica_groups=mesh['fs_0'=4,'fs_1'=4,'tp_0'=4,'tp_1'=2] {'fs_1'}, use_global_device_ids=true, to_apply=%region_4.0 | all-reduce | flops 1 | bytes 8 | tf_op jit(solution)/shard_map/psum | solution.py:62
  92.6 11.4 %psum.30 = f32[]{:T(128)} all-reduce(f32[]{:T(128)} %psum.29), channel_id=1, replica_groups=mesh['fs_0'=4,'fs_1'=4,'tp_0'=4,'tp_1'=2] {'tp_0'}, use_global_device_ids=true, to_apply=%region_5.0 | all-reduce | flops 1 | bytes 8 | tf_op jit(solution)/shard_map/psum | solution.py:62
  103.9 3.1 %psum.31 = f32[]{:T(128)} all-reduce(f32[]{:T(128)} %psum.30), channel_id=1, replica_groups=mesh['fs_0'=4,'fs_1'=4,'tp_0'=4,'tp_1'=2] {'tp_1'}, use_global_device_ids=true, to_apply=%region_6.0 | all-reduce | flops 1 | bytes 8 | tf_op jit(solution)/shard_map/psum | solution.py:62
  107.8 0.7 divide_convert_fusion.1
  108.5 21.7 %all_gather.6 = bf16[256,640]{1,0:T(8,128)(2,1)S(1)} all-gather(bf16[16,640]{1,0:T(8,128)(2,1)S(1)} %pad_maximum_fusion.3), channel_id=1, replica_groups=mesh['fs_0'=4,'fs_1'=4,'tp_0'=4,'tp_1'=2] {'fs_0','fs_1'}, dimensions={0}, use_global_device_ids=true | all-gather | bytes 348160 | tf_op jit(solution)/shard_map/all_gather | solution.py:69
  130.2 0.3 fusion.2
  130.6 1.0 fusion.7
  131.5 0.7 convert_bitcast_fusion
  132.2 0.7 pad_maximum_fusion.1
  132.9 46.4 %all-gather.2.cloned.1.call-done = bf16[2048,640]{0,1:T(8,128)(2,1)} async-done(((bf16[128,640]{0,1:T(8,128)(2,1)}), bf16[2048,640]{0,1:T(8,128)(2,1)}) %all-gather.2.cloned.1.call-update) | async-done | bytes 2621456 | tf_op jit(solution)/shard_map/all_gather | solution.py:77
  179.4 3.5 %slice_bitcast_fusion = (bf16[320,2048]{1,0:T(8,128)(2,1)}, bf16[2048,320]{0,1:T(8,128)(2,1)}) fusion(bf16[2048,640]{0,1:T(8,128)(2,1)} %all-gather.2.cloned.1.call-done), kind=kLoop, calls=%fused_computation.4 | loop fusion | bytes 5242880 | tf_op jit(solution)/shard_map/transpose | solution.py:81
  (32 shorter events, 0.5 us)
Async XLA Ops:
  7.2 46.1 %copy-start = (bf16[2048,320]{0,1:T(8,128)(2,1)S(1)}, bf16[2048,320]{0,1:T(8,128)(2,1)}, u32[]{:S(2)}) copy-start(bf16[2048,320]{0,1:T(8,128)(2,1)} %param.14) | copy-start | bytes 3932164
  7.2 172.2 %all-gather.2.cloned.1.call-start = ((), (), s32[]{:S(2)}) async-start(), calls=%async_computation.2 | async-start | bytes 2785280 | tf_op jit(solution)/shard_map/all_gather | solution.py:77
  8.4 42.4 %slice-start = ((s8[8388608]{0:T(1024)(128)(4,1)}), s8[4194304]{0:T(1024)(128)(4,1)S(1)}, s32[]{:S(2)}) async-start(s8[8388608]{0:T(1024)(128)(4,1)} %bitcast.25), calls=%async_computation.3 | async-start | bytes 8388608
  44.9 5.9 %slice-start.1 = ((s8[8388608]{0:T(1024)(128)(4,1)}), s8[4194304]{0:T(1024)(128)(4,1)S(1)}, s32[]{:S(2)}) async-start(s8[8388608]{0:T(1024)(128)(4,1)} %bitcast.25), calls=%async_computation.4 | async-start | bytes 8388608
  53.8 1.3 copy-start.1
  56.2 51.5 %copy-start.7 = (f32[16,320]{1,0:T(8,128)S(1)}, f32[16,320]{1,0:T(8,128)}, u32[]{:S(2)}) copy-start(f32[16,320]{1,0:T(8,128)} %param.21) | copy-start | bytes 61444
  56.2 51.5 %copy-start.8 = (f32[16,320]{1,0:T(8,128)S(1)}, f32[16,320]{1,0:T(8,128)}, u32[]{:S(2)}) copy-start(f32[16,320]{1,0:T(8,128)} %param.20) | copy-start | bytes 61444
  56.3 51.5 %copy-start.9 = (f32[16,320]{1,0:T(8,128)S(1)}, f32[16,320]{1,0:T(8,128)}, u32[]{:S(2)}) copy-start(f32[16,320]{1,0:T(8,128)} %param.23) | copy-start | bytes 61444
  56.3 51.5 %copy-start.10 = (f32[16,320]{1,0:T(8,128)S(1)}, f32[16,320]{1,0:T(8,128)}, u32[]{:S(2)}) copy-start(f32[16,320]{1,0:T(8,128)} %param.22) | copy-start | bytes 61444
  56.3 73.9 %copy-start.4 = (bf16[128,256]{1,0:T(8,128)(2,1)S(1)}, bf16[128,256]{1,0:T(8,128)(2,1)}, u32[]{:S(2)}) copy-start(bf16[128,256]{1,0:T(8,128)(2,1)} %param.17) | copy-start | bytes 196612
  56.3 74.2 %copy-start.3 = (bf16[128,256]{1,0:T(8,128)(2,1)S(1)}, bf16[128,256]{1,0:T(8,128)(2,1)}, u32[]{:S(2)}) copy-start(bf16[128,256]{1,0:T(8,128)(2,1)} %param.16) | copy-start | bytes 196612
  56.4 74.2 %copy-start.5 = (f32[128,320]{0,1:T(8,128)S(1)}, f32[128,320]{0,1:T(8,128)}, u32[]{:S(2)}) copy-start(f32[128,320]{0,1:T(8,128)} %param.18) | copy-start | bytes 491524
  56.6 74.9 %copy-start.6 = (f32[320,128]{1,0:T(8,128)S(1)}, f32[320,128]{1,0:T(8,128)}, u32[]{:S(2)}) copy-start(f32[320,128]{1,0:T(8,128)} %param.19) | copy-start | bytes 491524
  130.5 52.4 %copy-start.2 = (f32[320,128]{1,0:T(8,128)}, f32[320,128]{1,0:T(8,128)S(1)}, u32[]{:S(2)}) copy-start(f32[320,128]{1,0:T(8,128)S(1)} %fusion.2) | copy-start | bytes 491524
Sparse Core Ops, SparseCore 0:
  133.0 46.2 all-gather.1
where the time goes:
time: 190 us
  blocking collectives  106 us (56%)
  waiting for transfers between devices  46.5 us (24%)
  between operations  16.3 us (9%)
  matrix products  11.8 us (6%)
  local copies, waits for them, and re-layouts  4.78 us (3%)
  other arithmetic  3.89 us (2%)
    all_gather x1, waiting for transfers between devices, turned_gather(): filled = lax.all_gather(both, axis, axis=0, tiled=True)  46.4 us
    all_to_all x1, blocking collectives, sent_to_all(): return lax.all_to_all(copies, axis, split_axis=0, concat_axis=0, tiled=True)  36.4 us
    psum x4, blocking collectives, by_axis(): array = lax.psum(array, axis)  33.1 us
    all_gather x1, blocking collectives, in_one_piece_2(): filled = lax.all_gather(both, axis, axis=dim, tiled=True)  21.7 us
    all_to_all x1, blocking collectives, sent_and_summed(): lax.all_to_all(blocks, axis, split_axis=0, concat_axis=0, tiled=True)  15.2 us
    dot_general x2, matrix products, shards(): jnp.dot(pairs[number][0], wholes[number], preferred_element_type=jnp.floa...  8.31 us
  transfers between devices with their start and end apart: 1, of which 1 were waited for; matrix products, arithmetic and copies ran while one was open for 0% of the time, Pallas kernels for 0%

commit v1 on v0

--- a/solution.py
+++ b/solution.py
@@ -74,7 +74,9 @@
     turned = [jnp.moveaxis(a, dim, 0) for a, dim in zip(arrays, dims)]
     widths = [t[0].size for t in turned]
     both = jnp.concatenate([t.reshape(-1, w) for t, w in zip(turned, widths)], axis=1)
-    filled = lax.all_gather(both, axis, axis=0, tiled=True)
+    filled = jnp.concatenate(
+        lax.all_to_all(jnp.stack([both] * lax.axis_size(axis)), axis, 0, 0), axis=0
+    )
     blocks = jnp.split(filled, [sum(widths[:k]) for k in range(1, len(widths))], axis=1)
     return tuple(
         (

time: 190 us -> 173 us (0.911)
  waiting for transfers between devices: 46.5 us -> 0 us
  blocking collectives: 106 us -> 140 us
  between operations: 16.3 us -> 2.92 us
  local copies, waits for them, and re-layouts: 4.78 us -> 14.1 us
    all_gather x1 -> x0, waiting for transfers between devices: 46.4 us -> none  [turned_gather(): filled = lax.all_gather(both, axis, axis=0, tiled=True)]
    all_to_all x0 -> x1, blocking collectives: none -> 33.9 us  [turned_gather(): lax.all_to_all(jnp.stack([both] * lax.axis_size(axis)), axis, 0, 0)]
    all_to_all x0 -> x1, local copies, waits for them, and re-layouts: none -> 4.38 us  [turned_gather(): lax.all_to_all(jnp.stack([both] * lax.axis_size(axis)), axis, 0, 0)]
    unnamed x26 -> x28, local copies, waits for them, and re-layouts: 0.83 us -> 4.87 us
  transfers between devices with their start and end apart: 1 -> 0, of which waited for: 1 -> 0; matrix products, arithmetic and copies ran while one was open for 0% -> 0% of each run, Pallas kernels for 0% -> 0%
where the time goes in v1:
time: 173 us; the launch traced here: 172 us
  blocking collectives  140 us (81%)
  local copies, waits for them, and re-layouts  14.1 us (8%)
  matrix products  11.8 us (7%)
  other arithmetic  3.23 us (2%)
  between operations  2.92 us (2%)
    all_to_all x1, blocking collectives, sent_to_all(): return lax.all_to_all(copies, axis, split_axis=0, concat_axis=0, tiled=True)  36.4 us
    all_to_all x1, blocking collectives, turned_gather(): lax.all_to_all(jnp.stack([both] * lax.axis_size(axis)), axis, 0, 0)  33.9 us
    psum x4, blocking collectives, by_axis(): array = lax.psum(array, axis)  33.1 us
    all_gather x1, blocking collectives, in_one_piece_2(): filled = lax.all_gather(both, axis, axis=dim, tiled=True)  21.7 us
    all_to_all x1, blocking collectives, sent_and_summed(): lax.all_to_all(blocks, axis, split_axis=0, concat_axis=0, tiled=True)  15.3 us
    dot_general x2, matrix products, shards(): jnp.dot(pairs[number][0], wholes[number], preferred_element_type=jnp.floa...  8.31 us
    unnamed x28, local copies, waits for them, and re-layouts  4.87 us
    all_to_all x1, local copies, waits for them, and re-layouts, turned_gather(): lax.all_to_all(jnp.stack([both] * lax.axis_size(axis)), axis, 0, 0)  4.38 us

profile of v1, /device:TPU:0, one launch (start us, length us, event | category | flops | bytes accessed | tf_op | source)
XLA Modules:
  0.0 172.4 jit_solution(16301961745324588500)
XLA Ops:
  0.7 1.0 pad_maximum_fusion.2
  1.9 36.4 %all_to_all.15 = bf16[16,128,512]{2,1,0:T(8,128)(2,1)S(1)} all-to-all(bf16[16,128,512]{2,1,0:T(8,128)(2,1)S(1)} %broadcast_in_dim.3), channel_id=1, replica_groups=mesh['fs_0'=4,'fs_1'=4,'tp_0'=4,'tp_1'=2] {'fs_0','fs_1'}, dimensions={0} | all-to-all | bytes 4194304 | tf_op jit(solution)/shard_map/all_to_all | solution.py:23
  38.3 5.9 %fusion.10 = (bf16[2048,256]{0,1:T(8,128)(2,1)S(1)}, f32[2048,256]{0,1:T(8,128)S(1)}) fusion(bf16[2048,2048]{1,0:T(8,128)(2,1)} %param.15, bf16[2048,512]{1,0:T(8,128)(2,1)S(1)} %bitcast.25), kind=kOutput, calls=%fused_computation.33 | convolution fusion | flops 2148007936 | bytes 12582912 | tf_op jit(solution)/shard_map/dot_general | solution.py:124
  44.3 2.4 %fusion.11 = (bf16[2048,256]{0,1:T(8,128)(2,1)S(1)}, f32[2048,256]{0,1:T(8,128)S(1)}) fusion(bf16[2048,2048]{1,0:T(8,128)(2,1)S(1)} %bitcast.28, bf16[2048,512]{1,0:T(8,128)(2,1)S(1)} %bitcast.26), kind=kOutput, calls=%fused_computation.34 | convolution fusion | flops 2148007936 | bytes 12582912 | tf_op jit(solution)/shard_map/dot_general | solution.py:124
  46.7 0.5 fusion.13
  47.2 0.5 convolution_add_fusion
  47.8 0.8 copy-done.1
  48.5 0.5 fusion.12
  49.1 0.6 convolution_add_fusion.1
  50.1 15.3 %all_to_all.16 = f32[16,16,640]{2,1,0:T(8,128)S(1)} all-to-all(f32[16,16,640]{2,1,0:T(8,128)S(1)} %bitcast.24), channel_id=1, replica_groups=mesh['fs_0'=4,'fs_1'=4,'tp_0'=4,'tp_1'=2] {'fs_0','fs_1'}, dimensions={0} | all-to-all | bytes 1310720 | tf_op jit(solution)/shard_map/all_to_all | solution.py:47
  65.4 0.7 multiply_reduce_fusion
  67.4 9.1 %psum.28 = f32[]{:T(128)} all-reduce(f32[]{:T(128)S(6)} %add.42), channel_id=1, replica_groups=mesh['fs_0'=4,'fs_1'=4,'tp_0'=4,'tp_1'=2] {'fs_0'}, use_global_device_ids=true, to_apply=%region_3.0 | all-reduce | flops 1 | bytes 8 | tf_op jit(solution)/shard_map/psum | solution.py:62
  76.4 9.5 %psum.29 = f32[]{:T(128)} all-reduce(f32[]{:T(128)} %psum.28), channel_id=1, replica_groups=mesh['fs_0'=4,'fs_1'=4,'tp_0'=4,'tp_1'=2] {'fs_1'}, use_global_device_ids=true, to_apply=%region_4.0 | all-reduce | flops 1 | bytes 8 | tf_op jit(solution)/shard_map/psum | solution.py:62
  86.0 11.3 %psum.30 = f32[]{:T(128)} all-reduce(f32[]{:T(128)} %psum.29), channel_id=1, replica_groups=mesh['fs_0'=4,'fs_1'=4,'tp_0'=4,'tp_1'=2] {'tp_0'}, use_global_device_ids=true, to_apply=%region_5.0 | all-reduce | flops 1 | bytes 8 | tf_op jit(solution)/shard_map/psum | solution.py:62
  97.3 3.1 %psum.31 = f32[]{:T(128)} all-reduce(f32[]{:T(128)} %psum.30), channel_id=1, replica_groups=mesh['fs_0'=4,'fs_1'=4,'tp_0'=4,'tp_1'=2] {'tp_1'}, use_global_device_ids=true, to_apply=%region_6.0 | all-reduce | flops 1 | bytes 8 | tf_op jit(solution)/shard_map/psum | solution.py:62
  101.1 0.7 divide_convert_fusion.1
  101.9 21.7 %all_gather.3 = bf16[256,640]{1,0:T(8,128)(2,1)S(1)} all-gather(bf16[16,640]{1,0:T(8,128)(2,1)S(1)} %pad_maximum_fusion.3), channel_id=1, replica_groups=mesh['fs_0'=4,'fs_1'=4,'tp_0'=4,'tp_1'=2] {'fs_0','fs_1'}, dimensions={0}, use_global_device_ids=true | all-gather | bytes 348160 | tf_op jit(solution)/shard_map/all_gather | solution.py:69
  123.9 1.0 fusion.7
  124.9 0.7 convert_bitcast_fusion
  126.1 33.9 %all_to_all.17 = bf16[16,128,640]{1,2,0:T(8,128)(2,1)} all-to-all(bf16[16,128,640]{1,2,0:T(8,128)(2,1)S(1)} %stack.2), channel_id=1, replica_groups=mesh['fs_0'=4,'fs_1'=4,'tp_0'=4,'tp_1'=2] {'fs_0','fs_1'}, dimensions={0} | all-to-all | bytes 5242880 | tf_op jit(solution)/shard_map/all_to_all | solution.py:78
  160.1 4.4 %copy.25 = bf16[16,128,640]{2,1,0:T(8,128)(2,1)} copy(bf16[16,128,640]{1,2,0:T(8,128)(2,1)} %all_to_all.17) | data formatting | bytes 5242880 | tf_op jit(solution)/shard_map/all_to_all | solution.py:78
  164.5 3.9 %slice_bitcast_fusion = (bf16[320,2048]{0,1:T(8,128)(2,1)}, bf16[2048,320]{1,0:T(8,128)(2,1)S(1)}) fusion(bf16[2048,640]{1,0:T(8,128)(2,1)} %bitcast.23), kind=kLoop, calls=%fused_computation.4 | loop fusion | bytes 5242880 | tf_op jit(solution)/shard_map/transpose | solution.py:83
  168.4 2.5 %copy.27 = bf16[320,2048]{1,0:T(8,128)(2,1)} copy(bf16[320,2048]{0,1:T(8,128)(2,1)} %get-tuple-element.32) | data formatting | bytes 2621440
  170.9 1.5 copy.26
  (34 shorter events, 1.5 us)
Async XLA Ops:
  0.6 46.0 %copy-start = (bf16[2048,320]{0,1:T(8,128)(2,1)S(1)}, bf16[2048,320]{0,1:T(8,128)(2,1)}, u32[]{:S(2)}) copy-start(bf16[2048,320]{0,1:T(8,128)(2,1)} %param.14) | copy-start | bytes 3932164
  1.8 42.4 %slice-start = ((s8[8388608]{0:T(1024)(128)(4,1)}), s8[4194304]{0:T(1024)(128)(4,1)S(1)}, s32[]{:S(2)}) async-start(s8[8388608]{0:T(1024)(128)(4,1)} %bitcast.27), calls=%async_computation.3 | async-start | bytes 8388608
  38.3 5.9 %slice-start.1 = ((s8[8388608]{0:T(1024)(128)(4,1)}), s8[4194304]{0:T(1024)(128)(4,1)S(1)}, s32[]{:S(2)}) async-start(s8[8388608]{0:T(1024)(128)(4,1)} %bitcast.27), calls=%async_computation.4 | async-start | bytes 8388608
  47.2 1.3 copy-start.1
  49.7 51.4 %copy-start.7 = (f32[16,320]{1,0:T(8,128)S(1)}, f32[16,320]{1,0:T(8,128)}, u32[]{:S(2)}) copy-start(f32[16,320]{1,0:T(8,128)} %param.21) | copy-start | bytes 61444
  49.7 51.4 %copy-start.8 = (f32[16,320]{1,0:T(8,128)S(1)}, f32[16,320]{1,0:T(8,128)}, u32[]{:S(2)}) copy-start(f32[16,320]{1,0:T(8,128)} %param.20) | copy-start | bytes 61444
  49.7 51.4 %copy-start.9 = (f32[16,320]{1,0:T(8,128)S(1)}, f32[16,320]{1,0:T(8,128)}, u32[]{:S(2)}) copy-start(f32[16,320]{1,0:T(8,128)} %param.23) | copy-start | bytes 61444
  49.7 51.4 %copy-start.10 = (f32[16,320]{1,0:T(8,128)S(1)}, f32[16,320]{1,0:T(8,128)}, u32[]{:S(2)}) copy-start(f32[16,320]{1,0:T(8,128)} %param.22) | copy-start | bytes 61444
  49.8 73.8 %copy-start.4 = (bf16[128,256]{1,0:T(8,128)(2,1)S(1)}, bf16[128,256]{1,0:T(8,128)(2,1)}, u32[]{:S(2)}) copy-start(bf16[128,256]{1,0:T(8,128)(2,1)} %param.17) | copy-start | bytes 196612
  49.8 74.1 %copy-start.3 = (bf16[128,256]{1,0:T(8,128)(2,1)S(1)}, bf16[128,256]{1,0:T(8,128)(2,1)}, u32[]{:S(2)}) copy-start(bf16[128,256]{1,0:T(8,128)(2,1)} %param.16) | copy-start | bytes 196612
  49.8 74.1 %copy-start.5 = (f32[128,320]{0,1:T(8,128)S(1)}, f32[128,320]{0,1:T(8,128)}, u32[]{:S(2)}) copy-start(f32[128,320]{0,1:T(8,128)} %param.18) | copy-start | bytes 491524
  50.0 74.9 %copy-start.6 = (f32[320,128]{1,0:T(8,128)S(1)}, f32[320,128]{1,0:T(8,128)}, u32[]{:S(2)}) copy-start(f32[320,128]{1,0:T(8,128)} %param.19) | copy-start | bytes 491524
  123.9 2.2 %copy-start.2 = (f32[320,128]{1,0:T(8,128)}, f32[320,128]{1,0:T(8,128)S(1)}, u32[]{:S(2)}) copy-start(f32[320,128]{1,0:T(8,128)S(1)} %fusion.2) | copy-start | bytes 491524
